TPU v7x, 32 devices: a whole 2x2x4 slice. The times are simulated.
32 devices in a mesh: sp: 8 (over z, x), tp: 4 (over y, core).
Axes of the slice: x: 2, y: 2, z: 4, core: 2. Of those that a mesh axis runs over, the one named last changes fastest.
Arguments:
- queries: bfloat16 [6144, 2048], P('sp', 'tp'), may hold values from -110 to 110
- key_rows: bfloat16 [6144, 512], P('sp', 'tp'), may hold values from -4.5 to 4.5
- values: bfloat16 [6144, 512], P('sp', 'tp'), may hold values from -6 to 6
- sink_logits: float32 [32], P('tp'), may hold values from 2 to 7
- doc_ids: int32 [6144], P('sp'), may hold values from 0 to 3, as said below
- residual: bfloat16 [6144, 2048], P('sp'), may hold values from -20 to 20
- w_out: bfloat16 [2048, 2048], P('tp'), may hold values from -2.390625 to 2.390625
- norm_gain: float32 [2048], replicated, may hold values from 0.1 to 1.9
- w_value_up: bfloat16 [2048, 5632], P('sp', 'tp'), may hold values from -0.125 to 0.125
- w_gate_up: bfloat16 [2048, 5632], P('sp', 'tp'), may hold values from -0.125 to 0.125
- conv_taps: bfloat16 [3, 5632], P(None, 'tp'), may hold values from -3.5 to 3.5
- w_down_t: bfloat16 [2048, 5632], P('sp', 'tp'), may hold values from -0.078125 to 0.078125
Outputs:
- layer_out: bfloat16 [6144, 2048], P('sp', 'tp')
Inputs may be any that keep to these rules, and one draw needn't show every extreme that they name: `doc_ids`: document numbers never fall along the sequence and every one of the 4 documents is present; each document has 2 or more positions.
All inputs are finite; a program needn't handle non-finite values.
Results may differ from a plain program's by a relative error of at most 0.017.
Values may be sent and summed in bfloat16 or wider, within the bound.
A program may use at most 64 MiB of HBM per device.

v0:
```python
import jax
import jax.numpy as jnp
from jax import lax
from jax.sharding import PartitionSpec as P

HEAD_DIM = 64
WINDOW = 128


EPS = 1e-06
NEG = -1e30


def extended(block, sides, width):
    for axis, dim in sides:
        count = lax.axis_size(axis)
        forward = [(i, i + 1) for i in range(count - 1)]
        backward = [(target, source) for source, target in forward]
        low = lax.ppermute(
            lax.slice_in_dim(block, block.shape[dim] - width, None, axis=dim), axis, forward
        )
        high = lax.ppermute(lax.slice_in_dim(block, 0, width, axis=dim), axis, backward)
        block = jnp.concatenate([low, block, high], axis=dim)
    return block


def local_attention(queries, rim_kv, rim_labels, labels, sink_logits, kv_cols):
    rows_here = queries.shape[0]
    blocks = rows_here // WINDOW
    kv_local = kv_cols // HEAD_DIM
    heads_here = queries.shape[1] // HEAD_DIM
    per_kv = heads_here // kv_local
    kv_blocks = rim_kv.reshape(blocks + 2, WINDOW, rim_kv.shape[1])
    kv_window = jnp.concatenate([kv_blocks[:-2], kv_blocks[1:-1], kv_blocks[2:]], axis=1)
    lab_blocks = rim_labels.reshape(blocks + 2, WINDOW)
    doc_window = jnp.concatenate([lab_blocks[:-2], lab_blocks[1:-1], lab_blocks[2:]], axis=1)
    q_blocks = queries.reshape(blocks, WINDOW, kv_local, per_kv, HEAD_DIM)
    k_blocks = kv_window[:, :, :kv_cols].reshape(blocks, 3 * WINDOW, kv_local, HEAD_DIM)
    v_blocks = kv_window[:, :, kv_cols:].reshape(blocks, 3 * WINDOW, kv_local, HEAD_DIM)
    score = jnp.einsum(
        "nqkgd,njkd->nkgqj", q_blocks, k_blocks, preferred_element_type=jnp.float32
    ) * HEAD_DIM ** (-0.5)
    offsets = jnp.arange(3 * WINDOW)[None, :] - WINDOW - jnp.arange(WINDOW)[:, None]
    in_band = jnp.abs(offsets) <= WINDOW
    doc_query = labels.reshape(blocks, WINDOW)
    allowed = in_band[None] & (doc_query[:, :, None] == doc_window[:, None, :])
    allowed = allowed[:, None, None, :, :]
    sink_grid = sink_logits.reshape(kv_local, per_kv)[None, :, :, None]
    highest = jnp.maximum(jnp.max(jnp.where(allowed, score, NEG), axis=-1), sink_grid)
    raw = jnp.where(allowed, jnp.exp(score - highest[..., None]), 0.0)
    total = jnp.sum(raw, axis=-1) + jnp.exp(sink_grid - highest)
    probs = (raw / total[..., None]).astype(jnp.bfloat16)
    attended = jnp.einsum("nkgqj,njkd->nqkgd", probs, v_blocks, preferred_element_type=jnp.float32)
    return attended.reshape(rows_here, queries.shape[1]).astype(jnp.bfloat16)


def per_device(
    queries,
    key_rows,
    values,
    sink_logits,
    doc_ids,
    residual,
    w_out,
    norm_gain,
    w_value_up,
    w_gate_up,
    conv_taps,
    w_down_t,
):
    rows_here = queries.shape[0]
    model_width = residual.shape[1]
    span_cols = model_width // lax.axis_size("tp")
    first_col = lax.axis_index("tp") * span_cols
    kv_cols = key_rows.shape[1]
    stacked = jnp.concatenate([key_rows, values], axis=1)
    labels = doc_ids + 1
    rim_kv, rim_labels = (
        extended(stacked, (("sp", 0),), WINDOW),
        extended(labels, (("sp", 0),), WINDOW),
    )
    attended = local_attention(queries, rim_kv, rim_labels, labels, sink_logits, kv_cols)
    partial_value = jnp.dot(attended, w_out, preferred_element_type=jnp.float32)
    summed = lax.psum(partial_value.astype(jnp.bfloat16), "tp").astype(jnp.float32)
    mixed = (residual.astype(jnp.float32) + summed).astype(jnp.bfloat16)
    mixed_f = mixed.astype(jnp.float32)
    mean_sq = jnp.mean(mixed_f * mixed_f, axis=1, keepdims=True)
    normed = (mixed_f * lax.rsqrt(mean_sq + EPS) * norm_gain).astype(jnp.bfloat16)
    own_cols = lax.dynamic_slice_in_dim(mixed, first_col, span_cols, 1)
    value_f32 = jnp.dot(
        normed,
        lax.all_gather(w_value_up, "sp", axis=0, tiled=True),
        preferred_element_type=jnp.float32,
    )
    gate_f32 = jnp.dot(
        normed,
        lax.all_gather(w_gate_up, "sp", axis=0, tiled=True),
        preferred_element_type=jnp.float32,
    )
    up_value = value_f32.astype(jnp.bfloat16)
    up_gate = gate_f32.astype(jnp.bfloat16)
    rim_value = extended(up_value, (("sp", 0),), 1).astype(jnp.float32)
    prev_same = (rim_labels[WINDOW - 1 : WINDOW - 1 + rows_here] == labels)[:, None]
    next_same = (rim_labels[WINDOW + 1 : WINDOW + 1 + rows_here] == labels)[:, None]
    tap_f = conv_taps.astype(jnp.float32)
    conv = (
        tap_f[0] * jnp.where(prev_same, rim_value[:-2], 0.0)
        + tap_f[1] * up_value.astype(jnp.float32)
        + tap_f[2] * jnp.where(next_same, rim_value[2:], 0.0)
    )
    hidden = (jax.nn.silu(conv) * up_gate.astype(jnp.float32)).astype(jnp.bfloat16)
    partial_down = lax.dot_general(
        hidden,
        lax.all_gather(w_down_t, "sp", axis=0, tiled=True),
        (((1,), (1,)), ((), ())),
        preferred_element_type=jnp.float32,
    )
    ffn_cols = lax.psum_scatter(
        partial_down.astype(jnp.bfloat16), "tp", scatter_dimension=1, tiled=True
    ).astype(jnp.float32)
    return (own_cols.astype(jnp.float32) + ffn_cols).astype(jnp.bfloat16)


def solution(mesh):
    placed = (
        P("sp", "tp"),
        P("sp", "tp"),
        P("sp", "tp"),
        P("tp"),
        P("sp"),
        P("sp", None),
        P("tp", None),
        P(),
        P("sp", "tp"),
        P("sp", "tp"),
        P(None, "tp"),
        P("sp", "tp"),
    )
    return jax.shard_map(
        per_device, mesh=mesh, in_specs=placed, out_specs=P("sp", "tp"), check_vma=False
    )
```

profile of v0, /device:TPU:0, one launch (start us, length us, event | category | flops | bytes accessed | tf_op | source)
XLA Modules:
  0.0 392.3 jit_solution(13465538097866399492)
XLA Ops:
  7.4 0.0 copy-start
  7.4 0.0 all-reduce.2.cloned.1.call-start
  7.4 0.8 fusion.27
  8.2 4.9 %collective-permute-start.2 = (s32[128]{0:T(128)S(1)}, s32[128]{0:T(128)S(1)}, u32[]{:S(2)}, u32[]{:S(2)}) collective-permute-start(s32[128]{0:T(128)S(1)} %get-tuple-element.22), channel_id=1, source_target_pairs={{0,4},{4,8},{8,12},{12,16},{16,20},{20,24},{24,28},{1,5},{5,9},{9,... | collective-permute-start | bytes 1544 | tf_op jit(solution)/shard_map/ppermute | solution.py:19
  13.1 1.3 collective-permute-start.3
  14.4 1.0 constant_dynamic-update-slice_fusion.1
  15.4 1.0 constant_dynamic-update-slice_fusion
  16.3 4.5 %collective-permute-start = (bf16[128,256]{1,0:T(8,128)(2,1)S(1)}, bf16[128,256]{1,0:T(8,128)(2,1)S(1)}, u32[]{:S(2)}, u32[]{:S(2)}) collective-permute-start(bf16[128,256]{1,0:T(8,128)(2,1)S(1)} %get-tuple-element.16), channel_id=1, source_target_pairs={{0,4},{4,8},{8,12},{12,16},{16,20},{20,24},{24,28},{1,5},{5,9},{9,... | collective-permute-start | bytes 196616 | tf_op jit(solution)/shard_map/ppermute | solution.py:19
  20.9 1.3 collective-permute-start.1
  22.2 0.1 abs_compare_fusion
  22.3 0.2 copy.19
  22.6 3.6 reshape.95
  26.2 0.7 max.17
  26.9 0.0 collective-permute-done.2
  26.9 0.0 collective-permute-done.3
  27.0 0.5 compare_and_fusion
  27.5 0.0 collective-permute-done
  27.5 0.0 collective-permute-done.1
  27.5 0.9 pad_maximum_fusion.2
  28.4 1.2 copy.18
  29.6 1.9 copy.20
  31.6 0.0 copy-start.1
  31.6 1.3 pad_maximum_fusion
  32.8 0.1 fusion.29
  33.0 0.1 copy-done.1
  33.1 1.8 fusion
  34.9 0.1 broadcast_maximum_fusion
  34.9 2.3 fusion.3
  37.3 0.1 exponential_add_fusion
  37.4 2.8 fusion.17
  40.1 0.6 copy.24
  40.7 0.0 copy-done
  40.7 3.5 convolution_convert_fusion
  44.2 0.0 all-reduce.2.cloned.1.call-update
  44.2 0.0 all-gather.4.cloned.1.call-start
  44.2 0.5 all-gather.4.cloned.1.call-update
  44.8 0.0 all-gather.6.cloned.1.call-start
  44.8 0.5 all-gather.6.cloned.1.call-update
  45.4 0.0 all-gather.8.cloned.1.call-start
  45.4 0.5 all-gather.8.cloned.1.call-update
  45.9 0.2 reduce-scatter.2.cloned.1.call-start
  46.2 0.0 copy-done.4
  46.2 0.1 slice_reduce_fusion.2
  46.3 0.0 copy-start.5
  46.3 69.8 %all-reduce.2.cloned.1.call-done = bf16[768,2048]{1,0:T(8,128)(2,1)} async-done(((bf16[768,2048]{1,0:T(8,128)(2,1)}), bf16[768,2048]{1,0:T(8,128)(2,1)}) %all-reduce.2.cloned.1.call-update) | async-done | bytes 3145744 | tf_op jit(solution)/shard_map/psum | solution.py:84
  116.1 6.0 %fusion.4 = (f32[768]{0:T(1024)S(1)}, bf16[768,2048]{1,0:T(8,128)(2,1)}) fusion(bf16[768,2048]{1,0:T(8,128)(2,1)} %all-reduce.2.cloned.1.call-done, bf16[768,2048]{1,0:T(8,128)(2,1)} %param.17), kind=kLoop, calls=%fused_computation.9 | loop fusion | flops 11009280 | bytes 9440256 | tf_op jit(solution)/shard_map/reduce_sum | solution.py:87
  122.1 20.2 %all-gather.4.cloned.1.call-done = bf16[2048,1408]{1,0:T(8,128)(2,1)} async-done(((bf16[256,1408]{1,0:T(8,128)(2,1)}), bf16[2048,1408]{1,0:T(8,128)(2,1)}) %all-gather.4.cloned.1.call-update) | async-done | bytes 5767184 | tf_op jit(solution)/shard_map/all_gather | solution.py:92
  142.3 0.0 copy-done.5
  142.3 8.6 %convolution_convert_fusion.3 = bf16[768,1408]{1,0:T(8,128)(2,1)S(1)} fusion(bf16[2048,1408]{1,0:T(8,128)(2,1)} %all-gather.4.cloned.1.call-done, bf16[768,2048]{1,0:T(8,128)(2,1)} %get-tuple-element.9, f32[2048]{0:T(1024)S(1)} %copy-done.5, f32[768]{0:T(1024)S(1)} %add_rsqrt_fusion), kind=kOutput, calls=%fused_computation.24 | convolution fusion | flops 4436557824 | bytes 11086848 | tf_op jit(solution)/shard_map/dot_general | solution.py:90
  150.9 0.0 copy-start.2
  150.9 2.4 collective-permute-start.4
  153.4 1.3 collective-permute-start.5
  154.7 0.0 copy-done.3
  154.7 0.1 slice_compare_fusion.1
  154.8 0.0 collective-permute-done.4
  154.8 4.4 %collective-permute-done.5 = bf16[1,1408]{1,0:T(2,128)(2,1)S(1)} collective-permute-done((bf16[1,1408]{1,0:T(2,128)(2,1)S(1)}, bf16[1,1408]{1,0:T(2,128)(2,1)S(1)}, u32[]{:S(2)}, u32[]{:S(2)}) %collective-permute-start.5) | collective-permute-done | bytes 2848 | tf_op jit(solution)/shard_map/ppermute | solution.py:22
  159.1 0.0 copy-done.2
  159.1 2.5 maximum_convert_fusion
  161.7 73.1 %all-gather.6.cloned.1.call-done = bf16[2048,1408]{1,0:T(8,128)(2,1)} async-done(((bf16[256,1408]{1,0:T(8,128)(2,1)}), bf16[2048,1408]{1,0:T(8,128)(2,1)}) %all-gather.6.cloned.1.call-update) | async-done | bytes 5767184 | tf_op jit(solution)/shard_map/all_gather | solution.py:97
  234.8 92.3 %all-gather.8.cloned.1.call-done = bf16[2048,1408]{1,0:T(8,128)(2,1)} async-done(((bf16[256,1408]{1,0:T(8,128)(2,1)}), bf16[2048,1408]{1,0:T(8,128)(2,1)}) %all-gather.8.cloned.1.call-update) | async-done | bytes 5767184 | tf_op jit(solution)/shard_map/all_gather | solution.py:114
  327.1 19.1 %convolution_convert_fusion.1 = bf16[768,2048]{1,0:T(8,128)(2,1)} fusion(bf16[2048,1408]{1,0:T(8,128)(2,1)} %all-gather.8.cloned.1.call-done, f32[770,1408]{1,0:T(8,128)} %maximum_convert_fusion, bf16[768,1408]{1,0:T(8,128)(2,1)} %copy-done.2, f32[1408]{0:T(1024)S(1)} %get-tuple-element.6, f32[1408]{0:T(1024)S(1)} %get-tuple-element.7, ...), kind=kOutput, calls=%fused_computation.22 | convolution fusion | flops 8883535872 | bytes 28668928 | tf_op jit(solution)/shard_map/dot_general | solution.py:112
  346.2 0.0 reduce-scatter.2.cloned.1.call-update
  346.3 36.0 %reduce-scatter.2.cloned.1.call-done = bf16[768,512]{1,0:T(8,128)(2,1)} async-done(((bf16[768,2048]{1,0:T(8,128)(2,1)}), bf16[768,512]{1,0:T(8,128)(2,1)}) %reduce-scatter.2.cloned.1.call-update) | async-done | bytes 786448 | tf_op jit(solution)/shard_map/reduce_scatter | solution.py:118
  382.3 2.5 add_convert_fusion.1
  (11 shorter events, 0.1 us)
Async XLA Ops:
  7.4 33.3 %copy-start = (bf16[512,2048]{1,0:T(8,128)(2,1)S(1)}, bf16[512,2048]{1,0:T(8,128)(2,1)}, u32[]{:S(2)}) copy-start(bf16[512,2048]{1,0:T(8,128)(2,1)} %param.18) | copy-start | bytes 6291460
  7.4 108.7 %all-reduce.2.cloned.1.call-start = ((), (), s32[]{:S(2)}) async-start(), calls=%async_computation.1 | async-start | bytes 6291456 | tf_op jit(solution)/shard_map/psum | solution.py:84
  8.2 18.7 %collective-permute-start.2 = (s32[128]{0:T(128)S(1)}, s32[128]{0:T(128)S(1)}, u32[]{:S(2)}, u32[]{:S(2)}) collective-permute-start(s32[128]{0:T(128)S(1)} %get-tuple-element.22), channel_id=1, source_target_pairs={{0,4},{4,8},{8,12},{12,16},{16,20},{20,24},{24,28},{1,5},{5,9},{9,... | collective-permute-start | bytes 1544 | tf_op jit(solution)/shard_map/ppermute | solution.py:19
  13.1 13.9 %collective-permute-start.3 = (s32[128]{0:T(128)S(1)}, s32[128]{0:T(128)S(1)}, u32[]{:S(2)}, u32[]{:S(2)}) collective-permute-start(s32[128]{0:T(128)S(1)} %get-tuple-element.23), channel_id=1, source_target_pairs={{4,0},{8,4},{12,8},{16,12},{20,16},{24,20},{28,24},{5,1},{9,5},{13... | collective-permute-start | bytes 1544 | tf_op jit(solution)/shard_map/ppermute | solution.py:22
  16.3 11.1 %collective-permute-start = (bf16[128,256]{1,0:T(8,128)(2,1)S(1)}, bf16[128,256]{1,0:T(8,128)(2,1)S(1)}, u32[]{:S(2)}, u32[]{:S(2)}) collective-permute-start(bf16[128,256]{1,0:T(8,128)(2,1)S(1)} %get-tuple-element.16), channel_id=1, source_target_pairs={{0,4},{4,8},{8,12},{12,16},{16,20},{20,24},{24,28},{1,5},{5,9},{9,... | collective-permute-start | bytes 196616 | tf_op jit(solution)/shard_map/ppermute | solution.py:19
  20.9 6.6 %collective-permute-start.1 = (bf16[128,256]{1,0:T(8,128)(2,1)S(1)}, bf16[128,256]{1,0:T(8,128)(2,1)S(1)}, u32[]{:S(2)}, u32[]{:S(2)}) collective-permute-start(bf16[128,256]{1,0:T(8,128)(2,1)S(1)} %get-tuple-element.17), channel_id=1, source_target_pairs={{4,0},{8,4},{12,8},{16,12},{20,16},{24,20},{28,24},{5,1},{9,5},{13... | collective-permute-start | bytes 196616 | tf_op jit(solution)/shard_map/ppermute | solution.py:22
  31.6 1.5 copy-start.1
  44.2 2.0 copy-start.4
  44.2 98.1 %all-gather.4.cloned.1.call-start = ((), (), s32[]{:S(2)}) async-start(), calls=%async_computation.2 | async-start | bytes 6488064 | tf_op jit(solution)/shard_map/all_gather | solution.py:92
  44.8 190.0 %all-gather.6.cloned.1.call-start = ((), (), s32[]{:S(2)}) async-start(), calls=%async_computation.3 | async-start | bytes 6488064 | tf_op jit(solution)/shard_map/all_gather | solution.py:97
  45.4 281.8 %all-gather.8.cloned.1.call-start = ((), (), s32[]{:S(2)}) async-start(), calls=%async_computation.4 | async-start | bytes 6488064 | tf_op jit(solution)/shard_map/all_gather | solution.py:114
  45.9 336.3 %reduce-scatter.2.cloned.1.call-start = ((), (), s32[]{:S(2)}) async-start(), calls=%async_computation.5 | async-start | bytes 3932160 | tf_op jit(solution)/shard_map/reduce_scatter | solution.py:118
  46.3 96.0 %copy-start.5 = (f32[2048]{0:T(1024)S(1)}, f32[2048]{0:T(1024)}, u32[]{:S(2)}) copy-start(f32[2048]{0:T(1024)} %param.19) | copy-start | bytes 24580
  142.3 12.4 %copy-start.3 = (s32[768]{0:T(1024)S(1)}, s32[768]{0:T(1024)}, u32[]{:S(2)}) copy-start(s32[768]{0:T(1024)} %param.16) | copy-start | bytes 9220
  150.9 8.2 %copy-start.2 = (bf16[768,1408]{1,0:T(8,128)(2,1)}, bf16[768,1408]{1,0:T(8,128)(2,1)S(1)}, u32[]{:S(2)}) copy-start(bf16[768,1408]{1,0:T(8,128)(2,1)S(1)} %convolution_convert_fusion.3) | copy-start | bytes 6488068
  150.9 3.8 collective-permute-start.4
  153.4 5.8 %collective-permute-start.5 = (bf16[1,1408]{1,0:T(2,128)(2,1)S(1)}, bf16[1,1408]{1,0:T(2,128)(2,1)S(1)}, u32[]{:S(2)}, u32[]{:S(2)}) collective-permute-start(bf16[1,1408]{1,0:T(2,128)(2,1)S(1)} %get-tuple-element.11), channel_id=1, source_target_pairs={{4,0},{8,4},{12,8},{16,12},{20,16},{24,20},{28,24},{5,1},{9,5},{13... | collective-permute-start | bytes 8456 | tf_op jit(solution)/shard_map/ppermute | solution.py:22
Sparse Core Ops, SparseCore 0:
  44.3 71.7 all-reduce.1
  346.4 35.8 reduce-scatter.1
Sparse Core Ops, SparseCore 1:
  46.9 95.4 all-gather.3
  144.4 90.4 all-gather.5
  236.8 90.2 all-gather.7
where the time goes:
time: 393 us; the launch traced here: 392 us
  waiting for transfers between devices  297 us (76%)
  matrix products  35.7 us (9%)
  other arithmetic  17.2 us (4%)
  starting transfers between devices  16.1 us (4%)
  between operations  15.3 us (4%)
  local copies, waits for them, and re-layouts  10.6 us (3%)
    all_gather x1, waiting for transfers between devices, per_device(): lax.all_gather(w_down_t, 'sp', axis=0, tiled=True)  92.3 us
    all_gather x1, waiting for transfers between devices, per_device(): lax.all_gather(w_gate_up, 'sp', axis=0, tiled=True)  73.1 us
    psum x1, waiting for transfers between devices, per_device(): lax.psum(partial_value.astype(jnp.bfloat16), 'tp').astype(jnp.float32)  69.8 us
    reduce_scatter x1, waiting for transfers between devices, per_device(): lax.psum_scatter(partial_down.astype(jnp.bfloat16), 'tp', scatter_dimensi...  36 us
    all_gather x1, waiting for transfers between devices, per_device(): lax.all_gather(w_value_up, 'sp', axis=0, tiled=True)  20.2 us
    dot_general x1, matrix products, per_device(): lax.dot_general(hidden, lax.all_gather(w_down_t, 'sp', axis=0, tiled=True...  19.1 us
    ppermute x3, starting transfers between devices, extended(): lax.ppermute(lax.slice_in_dim(block, block.shape[dim] - width, None, axis...  11.9 us
    dot_general x1, matrix products, per_device(): jnp.dot(normed, lax.all_gather(w_value_up, 'sp', axis=0, tiled=True), pre...  8.59 us
  transfers between devices with their start and end apart: 11, of which 6 were waited for; matrix products, arithmetic and copies ran while one was open for 6% of the time, Pallas kernels for 0%

commit v1 on v0

v1 whole, which is shorter than its diff:
```python
import functools

import jax
import jax.numpy as jnp
from jax import lax
from jax.experimental import pallas as pl
from jax.experimental.pallas import tpu as pltpu
from jax.sharding import PartitionSpec as P

HEAD_DIM = 64
WINDOW = 128
EPS = 1e-06
NEG = -1e30
RIM = 16
MESH = pl.DeviceIdType.MESH
F32 = jnp.float32
BF16 = jnp.bfloat16


def kernel(
    n, ntp,
    q_ref, k_ref, v_ref, sink_ref, lab_row_ref, lab_col_ref, prev_ok_ref, next_ok_ref,
    res_hbm, wout_ref, gain_ref, wv_hbm, wg_hbm, taps_ref, wd_hbm,
    out_ref,
    up, down, kx, vx, lx, part, first, second, mixed, normed, value, gate, rim, pd, res,
    loc_sem, ring_send, ring_recv, halo_send, halo_recv, rim_send, rim_recv,
    core_send, core_recv, y_send, y_recv, back_send, back_recv, pair_send, pair_recv,
    dcore_send, dcore_recv, dy_send, dy_recv,
):
    me = lax.axis_index("sp")
    tp = lax.axis_index("tp")
    core = lax.rem(tp, 2)
    y = tp // 2
    ny = ntp // 2
    partner = y * 2 + 1 - core
    rows = q_ref.shape[0]
    half = rows // 2
    piece = half // ny
    block = wv_hbm.shape[0]
    depth = block // 2
    quarter = block // 4

    def place(p):
        h = p // (n // 2)
        return (1 - h) * (2 * p) + h * (2 * n - 1 - 2 * p)

    odd = lax.rem(me, 2)
    pos = (1 - odd) * (me // 2) + odd * ((2 * n - 1 - me) // 2)
    ahead = place(lax.rem(pos + 1, n))
    behind = place(lax.rem(pos + n - 1, n))
    right = lax.rem(me + 1, n)
    left = lax.rem(me + n - 1, n)

    loads = []
    for i, (src, dst) in enumerate((
        (wv_hbm, up.at[0, pl.ds(me * block, block)]),
        (wg_hbm, up.at[1, pl.ds(me * block, block)]),
        (wd_hbm, down.at[pl.ds(me * block, block)]),
        (res_hbm.at[pl.ds(core * half + y * piece, piece)], res),
    )):
        c = pltpu.make_async_copy(src, dst, loc_sem.at[i])
        c.start()
        loads.append(c)

    barrier = pltpu.get_barrier_semaphore()
    peers = [(ahead, tp), (behind, tp), (right, tp), (left, tp), (me, partner)]
    for j in range(1, ny):
        peers.append((me, lax.rem(y + j, ny) * 2 + core))
    for peer in peers:
        pl.semaphore_signal(barrier, inc=1, device_id=peer, device_id_type=MESH)
    for c in loads:
        c.wait()
    pl.semaphore_wait(barrier, len(peers))

    def spot(stream, way, owner):
        if stream < 2:
            return up.at[stream, pl.ds(owner * block + way * depth, depth)]
        return down.at[pl.ds(owner * block + way * depth + (stream - 2) * quarter, quarter)]

    def ring(stream, way, s, arriving):
        shift = s + 1 if arriving else s
        owner = place(lax.rem(pos + n - shift, n)) if way == 0 else place(lax.rem(pos + shift, n))
        ref = spot(stream, way, owner)
        return pltpu.make_async_remote_copy(
            src_ref=ref, dst_ref=ref,
            send_sem=ring_send.at[stream, way, s], recv_sem=ring_recv.at[stream, way, s],
            device_id=(ahead if way == 0 else behind, tp), device_id_type=MESH,
        )

    def begin(stream):
        for way in range(2):
            ring(stream, way, 0, False).start()

    def forward(stream, s, last=False):
        for way in range(2):
            ring(stream, way, s, True).wait_recv()
            if not last:
                ring(stream, way, s + 1, False).start()

    queue = []
    for s in range(n - 1):
        for stream in (0, 1):
            queue.append((stream, s))
    for s in range(n - 1):
        for stream in (2, 3):
            queue.append((stream, s))
    done = [0]

    def serve(count):
        for _ in range(count):
            if done[0] == len(queue):
                return
            stream, s = queue[done[0]]
            done[0] += 1
            forward(stream, s, last=s == n - 2)
            if stream < 2 and s == n - 2:
                begin(stream + 2)

    halo = []

    def remote(src, dst, send, recv, where):
        c = pltpu.make_async_remote_copy(
            src_ref=src, dst_ref=dst, send_sem=send, recv_sem=recv, device_id=where, device_id_type=MESH
        )
        c.start()
        return c

    ends = pl.ds(rows - WINDOW, WINDOW)
    starts = pl.ds(0, WINDOW)
    low, high = pl.ds(0, WINDOW), pl.ds(rows + WINDOW, WINDOW)
    for i, (src, dst) in enumerate(((k_ref, kx), (v_ref, vx))):
        halo.append(remote(src.at[ends], dst.at[low], halo_send.at[i, 0], halo_recv.at[i, 0], (right, tp)))
        halo.append(remote(src.at[starts], dst.at[high], halo_send.at[i, 1], halo_recv.at[i, 1], (left, tp)))
    halo.append(remote(lab_row_ref.at[:, ends], lx.at[:, low], halo_send.at[2, 0], halo_recv.at[2, 0], (right, tp)))
    halo.append(remote(lab_row_ref.at[:, starts], lx.at[:, high], halo_send.at[2, 1], halo_recv.at[2, 1], (left, tp)))
    begin(0)
    begin(1)
    inner = pl.ds(WINDOW, rows)
    kx[inner, :] = k_ref[...]
    vx[inner, :] = v_ref[...]
    lx[:, inner] = lab_row_ref[...]
    for c in halo:
        c.wait()

    kv_local = k_ref.shape[1] // HEAD_DIM
    per_kv = q_ref.shape[1] // k_ref.shape[1]
    blocks = rows // WINDOW
    model = wout_ref.shape[1]

    def attend(b, carry):
        here = pl.ds(pl.multiple_of(b * WINDOW, WINDOW), WINDOW)
        wide = pl.ds(pl.multiple_of(b * WINDOW, WINDOW), 3 * WINDOW)
        q = q_ref[here, :]
        kw = kx[wide, :]
        vw = vx[wide, :]
        lab_k = lx[0:1, wide]
        lab_q = lab_col_ref[here, :]
        key = lax.broadcasted_iota(jnp.int32, (WINDOW, 3 * WINDOW), 1) - WINDOW
        query = lax.broadcasted_iota(jnp.int32, (WINDOW, 3 * WINDOW), 0)
        at = key + me * rows + b * WINDOW
        allowed = (jnp.abs(key - query) <= WINDOW) & (lab_q == lab_k) & (at >= 0) & (at < n * rows)
        results = []
        for g in range(kv_local):
            k = kw[:, g * HEAD_DIM:(g + 1) * HEAD_DIM]
            v = vw[:, g * HEAD_DIM:(g + 1) * HEAD_DIM]
            for j in range(per_kv):
                h = g * per_kv + j
                qh = q[:, h * HEAD_DIM:(h + 1) * HEAD_DIM]
                score = lax.dot_general(
                    qh, k, (((1,), (1,)), ((), ())), preferred_element_type=F32
                ) * HEAD_DIM ** (-0.5)
                score = jnp.where(allowed, score, NEG)
                sink = sink_ref[h]
                highest = jnp.maximum(jnp.max(score, axis=1, keepdims=True), sink)
                raw = jnp.where(allowed, jnp.exp(score - highest), 0.0)
                total = jnp.sum(raw, axis=1, keepdims=True) + jnp.exp(sink - highest)
                probs = (raw / total).astype(BF16)
                results.append(jnp.dot(probs, v, preferred_element_type=F32).astype(BF16))
        attended = jnp.concatenate(results, axis=1)
        part[here, :] = jnp.dot(attended, wout_ref[...], preferred_element_type=F32).astype(BF16)
        return carry

    split = blocks // 3
    for t in range(3):
        lax.fori_loop(t * split, (t + 1) * split if t < 2 else blocks, attend, 0)
        serve(1)

    tile = 32
    other_half = pl.ds((1 - core) * half, half)
    swap = remote(part.at[other_half], first, core_send, core_recv, (me, partner))
    swap.wait()

    def add_first(i, carry):
        r = pl.ds(pl.multiple_of(i * tile, tile), tile)
        o = pl.ds(pl.multiple_of(core * half + i * tile, tile), tile)
        first[r, :] = (part[o, :].astype(F32) + first[r, :].astype(F32)).astype(BF16)
        return carry

    lax.fori_loop(0, half // tile, add_first, 0)
    copies = []
    for j in range(1, ny):
        to = lax.rem(y + j, ny)
        copies.append(remote(
            first.at[pl.ds(to * piece, piece)], second.at[j - 1], y_send.at[j - 1], y_recv.at[j - 1], (me, to * 2 + core)
        ))
    serve(2)
    for c in copies:
        c.wait()

    def add_second(i, carry):
        r = pl.ds(pl.multiple_of(i * tile, tile), tile)
        s = first[pl.ds(pl.multiple_of(y * piece + i * tile, tile), tile), :].astype(F32)
        for j in range(ny - 1):
            s = s + second[j, r, :].astype(F32)
        o = pl.ds(pl.multiple_of(core * half + y * piece + i * tile, tile), tile)
        mixed[o, :] = (res[r, :].astype(F32) + s).astype(BF16)
        return carry

    lax.fori_loop(0, piece // tile, add_second, 0)
    mine = mixed.at[pl.ds(core * half + y * piece, piece)]
    copies = []
    for j in range(1, ny):
        to = lax.rem(y + j, ny)
        copies.append(remote(mine, mine, back_send.at[j - 1], back_recv.at[j - 1], (me, to * 2 + core)))
    serve(2)
    for j, c in enumerate(copies):
        c.wait_send()
        frm = lax.rem(y + ny - (j + 1), ny)
        theirs = mixed.at[pl.ds(core * half + frm * piece, piece)]
        pltpu.make_async_remote_copy(
            src_ref=theirs, dst_ref=theirs, send_sem=back_send.at[j], recv_sem=back_recv.at[j],
            device_id=(me, partner), device_id_type=MESH,
        ).wait_recv()
    own_half = mixed.at[pl.ds(core * half, half)]
    swap = remote(own_half, own_half, pair_send, pair_recv, (me, partner))
    swap.wait_send()
    their_half = mixed.at[other_half]
    pltpu.make_async_remote_copy(
        src_ref=their_half, dst_ref=their_half, send_sem=pair_send, recv_sem=pair_recv,
        device_id=(me, partner), device_id_type=MESH,
    ).wait_recv()

    def normalise(i, carry):
        r = pl.ds(pl.multiple_of(i * tile, tile), tile)
        m = mixed[r, :].astype(F32)
        mean_sq = jnp.mean(m * m, axis=1, keepdims=True)
        normed[r, :] = (m * lax.rsqrt(mean_sq + EPS) * gain_ref[...]).astype(BF16)
        return carry

    lax.fori_loop(0, rows // tile, normalise, 0)

    serve(2 * (n - 1) - done[0])
    big = rows // 3

    def project(i, carry):
        r = pl.ds(pl.multiple_of(i * big, big), big)
        value[r, :] = jnp.dot(normed[r, :], up[0], preferred_element_type=F32).astype(BF16)
        gate[r, :] = jnp.dot(normed[r, :], up[1], preferred_element_type=F32).astype(BF16)
        return carry

    for t in range(3):
        lax.fori_loop(t, t + 1, project, 0)
        serve(2)

    tail = remote(value.at[pl.ds(rows - RIM, RIM)], rim.at[0], rim_send.at[0], rim_recv.at[0], (right, tp))
    head = remote(value.at[pl.ds(0, RIM)], rim.at[1], rim_send.at[1], rim_recv.at[1], (left, tp))
    tail.wait()
    head.wait()
    serve(1)

    taps = taps_ref[...].astype(F32)
    step = 64
    before = rim[0, RIM - 1:RIM, :].astype(F32)
    for i in range(rows // step):
        r = slice(i * step, (i + 1) * step)
        x = value[r, :].astype(F32)
        after = (value[(i + 1) * step:(i + 1) * step + RIM, :] if (i + 1) * step < rows else rim[1, :, :])[0:1].astype(F32)
        prev = jnp.concatenate([before, x[:-1]], axis=0)
        nxt = jnp.concatenate([x[1:], after], axis=0)
        conv = (
            taps[0:1] * jnp.where(prev_ok_ref[r, :] > 0, prev, 0.0)
            + taps[1:2] * x
            + taps[2:3] * jnp.where(next_ok_ref[r, :] > 0, nxt, 0.0)
        )
        gate[r, :] = (conv * jax.nn.sigmoid(conv) * gate[r, :].astype(F32)).astype(BF16)
        before = x[step - 1:step]
        if i % 4 == 3:
            serve(1)
    serve(len(queue))

    span = model // ntp

    def lower(t):
        def body(i, carry):
            r = pl.ds(pl.multiple_of(i * big, big), big)
            w = down[pl.ds(pl.multiple_of(t * span, span), span), :]
            pd[t, r, :] = lax.dot_general(
                gate[r, :], w, (((1,), (1,)), ((), ())), preferred_element_type=F32
            ).astype(BF16)
            return carry

        lax.fori_loop(0, 3, body, 0)

    inbox = part
    across = []
    for j in range(1, ny + 1):
        yy = lax.rem(y + j, ny)
        t = yy * 2 + 1 - core
        lower(t)
        across.append(remote(pd.at[t], second_in(inbox, yy, span), dcore_send.at[j - 1], dcore_recv.at[j - 1], (me, partner)))
    copies = []
    for j in range(1, ny + 1):
        yy = lax.rem(y + j, ny)
        t = yy * 2 + core
        lower(t)
        across[j - 1].wait()
        box = second_in(inbox, yy, span)

        def merge(i, carry):
            r = pl.ds(pl.multiple_of(i * 64, 64), 64)
            pd[t, r, :] = (pd[t, r, :].astype(F32) + box[r, :].astype(F32)).astype(BF16)
            return carry

        lax.fori_loop(0, rows // 64, merge, 0)
        if j < ny:
            to = yy * 2 + core
            copies.append(remote(
                pd.at[t], part.at[:, pl.ds((ny + j - 1) * span, span)], dy_send.at[j - 1], dy_recv.at[j - 1], (me, to)
            ))
    for c in copies:
        c.wait()

    def finish(i, carry):
        r = pl.ds(pl.multiple_of(i * 64, 64), 64)
        s = pd[tp, r, :].astype(F32)
        for j in range(ny - 1):
            s = s + part[r, (ny + j) * span:(ny + j + 1) * span].astype(F32)
        out_ref[r, :] = (mixed[r, pl.ds(pl.multiple_of(tp * span, span), span)].astype(F32) + s).astype(BF16)
        return carry

    lax.fori_loop(0, rows // 64, finish, 0)
    for stream in range(4):
        for way in range(2):
            for s in range(n - 1):
                ring(stream, way, s, False).wait_send()


def second_in(ref, slot, span):
    return ref.at[:, pl.ds(pl.multiple_of(slot * span, span), span)]


def solution(mesh):
    n, ntp = mesh.shape["sp"], mesh.shape["tp"]

    def per_device(q, k, v, sink, doc, res, wout, gain, wv, wg, taps, wd):
        rows, model = res.shape
        hidden = wv.shape[1]
        block = wv.shape[0]
        ny = ntp // 2
        edge_fwd = [(i, i + 1) for i in range(n - 1)]
        edge_bwd = [(b, a) for a, b in edge_fwd]
        labels = doc + 1
        before = lax.ppermute(labels[-1:], "sp", edge_fwd)
        after = lax.ppermute(labels[:1], "sp", edge_bwd)
        padded = jnp.concatenate([before, labels, after])
        prev_ok = (padded[:-2] == labels).astype(F32)[:, None]
        next_ok = (padded[2:] == labels).astype(F32)[:, None]
        lab_row = jnp.broadcast_to(labels[None, :], (8, rows))
        vm = pl.BlockSpec(memory_space=pltpu.VMEM)
        hbm = pl.BlockSpec(memory_space=pl.ANY)
        smem = pl.BlockSpec(memory_space=pltpu.SMEM)
        dma = pltpu.SemaphoreType.DMA
        kvc = k.shape[1]
        span = model // ntp
        scratch = [
            pltpu.VMEM((2, n * block, hidden), BF16),
            pltpu.VMEM((n * block, hidden), BF16),
            pltpu.VMEM((rows + 2 * WINDOW, kvc), BF16),
            pltpu.VMEM((rows + 2 * WINDOW, kvc), BF16),
            pltpu.VMEM((8, rows + 2 * WINDOW), jnp.int32),
            pltpu.VMEM((rows, model), BF16),
            pltpu.VMEM((rows // 2, model), BF16),
            pltpu.VMEM((max(ny - 1, 1), rows // 2 // ny, model), BF16),
            pltpu.VMEM((rows, model), BF16),
            pltpu.VMEM((rows, model), BF16),
            pltpu.VMEM((rows, hidden), BF16),
            pltpu.VMEM((rows, hidden), BF16),
            pltpu.VMEM((2, RIM, hidden), BF16),
            pltpu.VMEM((ntp, rows, span), BF16),
            pltpu.VMEM((rows // 2 // ny, model), BF16),
            dma((4,)),
            dma((4, 2, n - 1)), dma((4, 2, n - 1)),
            dma((3, 2)), dma((3, 2)),
            dma((2,)), dma((2,)),
            dma, dma,
            dma((ny,)), dma((ny,)),
            dma((ny,)), dma((ny,)),
            dma, dma,
            dma((ny,)), dma((ny,)),
            dma((ny,)), dma((ny,)),
        ]
        return pl.pallas_call(
            functools.partial(kernel, n, ntp),
            out_shape=jax.ShapeDtypeStruct((rows, span), BF16),
            in_specs=[vm, vm, vm, smem, vm, vm, vm, vm, hbm, vm, vm, hbm, hbm, vm, hbm],
            out_specs=vm,
            scratch_shapes=scratch,
            compiler_params=pltpu.CompilerParams(
                collective_id=0, has_side_effects=True, vmem_limit_bytes=67043328
            ),
            name="layer",
        )(q, k, v, sink, lab_row, labels[:, None], prev_ok, next_ok, res, wout, gain[None, :], wv, wg, taps, wd)

    placed = (
        P("sp", "tp"), P("sp", "tp"), P("sp", "tp"), P("tp"), P("sp"), P("sp", None),
        P("tp", None), P(), P("sp", "tp"), P("sp", "tp"), P(None, "tp"), P("sp", "tp"),
    )
    return jax.shard_map(
        per_device, mesh=mesh, in_specs=placed, out_specs=P("sp", "tp"), check_vma=False
    )
```

time: 393 us -> 226 us (0.58)
  waiting for transfers between devices: 297 us -> 0.08 us
  Pallas kernels: 0 us -> 209 us
  matrix products: 35.7 us -> 0 us
  between operations: 15.3 us -> 0.02 us
  other arithmetic: 17.2 us -> 2.77 us
  starting transfers between devices: 16.1 us -> 7.28 us
  local copies, waits for them, and re-layouts: 10.6 us -> 6.02 us
    pallas_call x0 -> x1, Pallas kernels: none -> 209 us  [per_device(): pl.pallas_call(functools.partial(kernel, n, ntp), out_shape=jax.ShapeDtyp...]
    all_gather x3 -> x0, waiting for transfers between devices: 186 us -> none  [the longest x1 92.3 us: per_device(): lax.all_gather(w_down_t, 'sp', axis=0, tiled=True)]
    psum x1 -> x0, waiting for transfers between devices: 69.8 us -> none  [per_device(): lax.psum(partial_value.astype(jnp.bfloat16), 'tp').astype(jnp.float32)]
    reduce_scatter x1 -> x0, waiting for transfers between devices: 36 us -> none  [per_device(): lax.psum_scatter(partial_down.astype(jnp.bfloat16), 'tp', scatter_dimensi...]
    dot_general x5 -> x0, matrix products: 35.7 us -> none  [the longest x1 19.1 us: per_device(): lax.dot_general(hidden, lax.all_gather(w_down_t, 'sp', axis=0, tiled=True...]
    ppermute x6 -> x2, starting transfers between devices: 15.7 us -> 7.28 us  [the longest x1 6 us: per_device(): before = lax.ppermute(labels[-1:], 'sp', edge_fwd)]
    reduce_sum x2 -> x0, other arithmetic: 8.35 us -> none  [the longest x1 6.02 us: per_device(): mean_sq = jnp.mean(mixed_f * mixed_f, axis=1, keepdims=True)]
    convert_element_type x3 -> x0, other arithmetic: 4.98 us -> none  [the longest x1 2.52 us: per_device(): rim_value = extended(up_value, (('sp', 0),), 1).astype(jnp.float32)]
  transfers between devices with their start and end apart: 11 -> 2, of which waited for: 6 -> 1; matrix products, arithmetic and copies ran while one was open for 6% -> 0% of each run, Pallas kernels for 0% -> 0%
where the time goes in v1:
time: 226 us
  Pallas kernels  209 us (92%)
  starting transfers between devices  7.28 us (3%)
  local copies, waits for them, and re-layouts  6.02 us (3%)
  other arithmetic  2.77 us (1%)
    pallas_call x1, Pallas kernels, per_device(): pl.pallas_call(functools.partial(kernel, n, ntp), out_shape=jax.ShapeDtyp...  209 us
    ppermute x1, starting transfers between devices, per_device(): before = lax.ppermute(labels[-1:], 'sp', edge_fwd)  6 us
  transfers between devices with their start and end apart: 2, of which 1 were waited for; matrix products, arithmetic and copies ran while one was open for 0% of the time, Pallas kernels for 0%

profile of v1, /device:TPU:0, one launch (start us, length us, event | category | flops | bytes accessed | tf_op | source)
XLA Modules:
  0.0 225.6 jit_solution(6956920817324704480)
XLA Ops:
  0.0 0.7 broadcast_add_fusion
  0.7 0.6 fusion.2
  1.3 1.3 collective-permute-start.1
  2.6 6.0 %collective-permute-start = (s32[1]{0:T(128)}, s32[1]{0:T(128)}, u32[]{:S(2)}, u32[]{:S(2)}) collective-permute-start(s32[1]{0:T(128)} %get-tuple-element.10), channel_id=1, source_target_pairs={{0,4},{4,8},{8,12},{12,16},{16,20},{20,24},{24,28},{1,5},{5,9},{9,... | collective-permute-start | bytes 20 | tf_op jit(solution)/shard_map/ppermute | solution.py:363
  8.6 0.9 broadcast_in_dim.31.lab_col_ref
  9.5 0.0 collective-permute-done.1
  9.5 0.1 collective-permute-done
  9.6 1.3 pad_add_fusion.1
  10.9 0.8 fusion.1
  11.6 0.9 reshape.4.next_ok_ref
  12.6 0.9 reshape.3.prev_ok_ref
  13.5 0.6 broadcast_in_dim.22.lab_row_ref
  14.1 209.4 %layer.1 = bf16[768,512]{1,0:T(8,128)(2,1)} custom-call(bf16[768,512]{1,0:T(8,128)(2,1)} %q_ref.1, bf16[768,128]{1,0:T(8,128)(2,1)} %k_ref.1, bf16[768,128]{1,0:T(8,128)(2,1)} %v_ref.1, f32[8]{0:T(128)} %sink_ref.1, s32[8,768]{1,0:T(8,128)} %broadcast_in_dim.22.lab_row_ref, s32[768,1]{1,0:T(8,128)} %broadcast_in_dim.31.lab_col_ref, ...), custom_call_target="tpu_custom_call" | custom-call | tf_op jit(solution)/shard_map/layer/pallas_call | solution.py:402
  223.5 2.1 copy.17
Async XLA Ops:
  1.3 8.2 %collective-permute-start.1 = (s32[1]{0:T(128)}, s32[1]{0:T(128)}, u32[]{:S(2)}, u32[]{:S(2)}) collective-permute-start(s32[1]{0:T(128)} %get-tuple-element.9), channel_id=1, source_target_pairs={{4,0},{8,4},{12,8},{16,12},{20,16},{24,20},{28,24},{5,1},{9,5},{13... | collective-permute-start | bytes 20 | tf_op jit(solution)/shard_map/ppermute | solution.py:364
  2.6 7.0 %collective-permute-start = (s32[1]{0:T(128)}, s32[1]{0:T(128)}, u32[]{:S(2)}, u32[]{:S(2)}) collective-permute-start(s32[1]{0:T(128)} %get-tuple-element.10), channel_id=1, source_target_pairs={{0,4},{4,8},{8,12},{12,16},{16,20},{20,24},{24,28},{1,5},{5,9},{9,... | collective-permute-start | bytes 20 | tf_op jit(solution)/shard_map/ppermute | solution.py:363

commit v2 on v1

--- a/solution.py
+++ b/solution.py
@@ -19,13 +19,13 @@
 
 def kernel(
     n, ntp,
-    q_ref, k_ref, v_ref, sink_ref, lab_row_ref, lab_col_ref, prev_ok_ref, next_ok_ref,
+    q_ref, k_ref, v_ref, sink_ref, lab_row_ref,
     res_hbm, wout_ref, gain_ref, wv_hbm, wg_hbm, taps_ref, wd_hbm,
     out_ref,
-    up, down, kx, vx, lx, part, first, second, mixed, normed, value, gate, rim, pd, res,
+    up, down, kx, vx, lx, lc, part, first, second, mixed, normed, value, gate, rim, pd, box, inbox, res,
     loc_sem, ring_send, ring_recv, halo_send, halo_recv, rim_send, rim_recv,
     core_send, core_recv, y_send, y_recv, back_send, back_recv, pair_send, pair_recv,
-    dcore_send, dcore_recv, dy_send, dy_recv,
+    down_send, down_recv, out_send, out_recv,
 ):
     me = lax.axis_index("sp")
     tp = lax.axis_index("tp")
@@ -63,9 +63,9 @@
         loads.append(c)
 
     barrier = pltpu.get_barrier_semaphore()
-    peers = [(ahead, tp), (behind, tp), (right, tp), (left, tp), (me, partner)]
-    for j in range(1, ny):
-        peers.append((me, lax.rem(y + j, ny) * 2 + core))
+    peers = [(ahead, tp), (behind, tp), (right, tp), (left, tp)]
+    for j in range(1, ntp):
+        peers.append((me, lax.rem(tp + j, ntp)))
     for peer in peers:
         pl.semaphore_signal(barrier, inc=1, device_id=peer, device_id_type=MESH)
     for c in loads:
@@ -141,6 +141,12 @@
     lx[:, inner] = lab_row_ref[...]
     for c in halo:
         c.wait()
+    lx[:, low] = jnp.where(me == 0, -1, lx[:, low])
+    lx[:, high] = jnp.where(me == n - 1, -1, lx[:, high])
+    for i in range(rows // WINDOW + 2):
+        chunk = slice(i * WINDOW, (i + 1) * WINDOW)
+        square = jnp.broadcast_to(lx[0:1, chunk].astype(F32), (WINDOW, WINDOW))
+        lc[chunk, :] = jnp.transpose(square)
 
     kv_local = k_ref.shape[1] // HEAD_DIM
     per_kv = q_ref.shape[1] // k_ref.shape[1]
@@ -153,12 +159,11 @@
         q = q_ref[here, :]
         kw = kx[wide, :]
         vw = vx[wide, :]
-        lab_k = lx[0:1, wide]
-        lab_q = lab_col_ref[here, :]
+        lab_k = lx[0:1, wide].astype(F32)
+        lab_q = lc[pl.ds(pl.multiple_of(b * WINDOW + WINDOW, WINDOW), WINDOW), 0:1]
         key = lax.broadcasted_iota(jnp.int32, (WINDOW, 3 * WINDOW), 1) - WINDOW
         query = lax.broadcasted_iota(jnp.int32, (WINDOW, 3 * WINDOW), 0)
-        at = key + me * rows + b * WINDOW
-        allowed = (jnp.abs(key - query) <= WINDOW) & (lab_q == lab_k) & (at >= 0) & (at < n * rows)
+        allowed = (jnp.abs(key - query) <= WINDOW) & (lab_q == lab_k)
         results = []
         for g in range(kv_local):
             k = kw[:, g * HEAD_DIM:(g + 1) * HEAD_DIM]
@@ -252,25 +257,28 @@
     serve(2 * (n - 1) - done[0])
     big = rows // 3
 
-    def project(i, carry):
-        r = pl.ds(pl.multiple_of(i * big, big), big)
-        value[r, :] = jnp.dot(normed[r, :], up[0], preferred_element_type=F32).astype(BF16)
-        gate[r, :] = jnp.dot(normed[r, :], up[1], preferred_element_type=F32).astype(BF16)
-        return carry
+    def project(t, which, dst):
+        r = slice(t * big, (t + 1) * big)
+        dst[r, :] = jnp.dot(normed[r, :], up[which], preferred_element_type=F32).astype(BF16)
 
     for t in range(3):
-        lax.fori_loop(t, t + 1, project, 0)
-        serve(2)
-
+        project(t, 0, value)
+        serve(1)
     tail = remote(value.at[pl.ds(rows - RIM, RIM)], rim.at[0], rim_send.at[0], rim_recv.at[0], (right, tp))
     head = remote(value.at[pl.ds(0, RIM)], rim.at[1], rim_send.at[1], rim_recv.at[1], (left, tp))
+    for t in range(3):
+        project(t, 1, gate)
+        serve(1)
     tail.wait()
     head.wait()
-    serve(1)
 
     taps = taps_ref[...].astype(F32)
     step = 64
     before = rim[0, RIM - 1:RIM, :].astype(F32)
+
+    def label(i, shift):
+        return lc[WINDOW + i * step + shift:WINDOW + (i + 1) * step + shift, 0:1]
+
     for i in range(rows // step):
         r = slice(i * step, (i + 1) * step)
         x = value[r, :].astype(F32)
@@ -278,75 +286,110 @@
         prev = jnp.concatenate([before, x[:-1]], axis=0)
         nxt = jnp.concatenate([x[1:], after], axis=0)
         conv = (
-            taps[0:1] * jnp.where(prev_ok_ref[r, :] > 0, prev, 0.0)
+            taps[0:1] * jnp.where(label(i, -1) == label(i, 0), prev, 0.0)
             + taps[1:2] * x
-            + taps[2:3] * jnp.where(next_ok_ref[r, :] > 0, nxt, 0.0)
+            + taps[2:3] * jnp.where(label(i, 1) == label(i, 0), nxt, 0.0)
         )
         gate[r, :] = (conv * jax.nn.sigmoid(conv) * gate[r, :].astype(F32)).astype(BF16)
         before = x[step - 1:step]
         if i % 4 == 3:
             serve(1)
-    serve(len(queue))
-
-    span = model // ntp
-
-    def lower(t):
+
+    per_tp = n // ntp
+    mine_rows = pl.ds(core * half, half)
+    partner_rows = pl.ds((1 - core) * half, half)
+    need = {d: 2 * (n - 1) + (2 * max(d, n - d) if d else 0) for d in range(n)}
+    order = sorted(range(n), key=lambda d: need[d])
+
+    def target(owner):
+        to = owner // per_tp
+        local = lax.rem(owner, per_tp)
+        slot = lax.rem(tp - to + ntp, ntp) - 1
+        return to, local, slot
+
+    def lower(d):
+        owner = place(lax.rem(pos + d, n))
+        w = down[pl.ds(pl.multiple_of(owner * block, block), block), :]
+
         def body(i, carry):
             r = pl.ds(pl.multiple_of(i * big, big), big)
-            w = down[pl.ds(pl.multiple_of(t * span, span), span), :]
-            pd[t, r, :] = lax.dot_general(
+            pd[owner, r, :] = lax.dot_general(
                 gate[r, :], w, (((1,), (1,)), ((), ())), preferred_element_type=F32
             ).astype(BF16)
             return carry
 
         lax.fori_loop(0, 3, body, 0)
-
-    inbox = part
-    across = []
-    for j in range(1, ny + 1):
-        yy = lax.rem(y + j, ny)
-        t = yy * 2 + 1 - core
-        lower(t)
-        across.append(remote(pd.at[t], second_in(inbox, yy, span), dcore_send.at[j - 1], dcore_recv.at[j - 1], (me, partner)))
-    copies = []
-    for j in range(1, ny + 1):
-        yy = lax.rem(y + j, ny)
-        t = yy * 2 + core
-        lower(t)
-        across[j - 1].wait()
-        box = second_in(inbox, yy, span)
+        return remote(
+            pd.at[owner, partner_rows], box.at[owner], down_send.at[d], down_recv.at[d], (me, partner)
+        )
+
+    def reduce(d, c):
+        owner = place(lax.rem(pos + d, n))
+        c.wait()
 
         def merge(i, carry):
-            r = pl.ds(pl.multiple_of(i * 64, 64), 64)
-            pd[t, r, :] = (pd[t, r, :].astype(F32) + box[r, :].astype(F32)).astype(BF16)
+            r = pl.ds(pl.multiple_of(i * tile, tile), tile)
+            o = pl.ds(pl.multiple_of(core * half + i * tile, tile), tile)
+            pd[owner, o, :] = (pd[owner, o, :].astype(F32) + box[owner, r, :].astype(F32)).astype(BF16)
             return carry
 
-        lax.fori_loop(0, rows // 64, merge, 0)
-        if j < ny:
-            to = yy * 2 + core
-            copies.append(remote(
-                pd.at[t], part.at[:, pl.ds((ny + j - 1) * span, span)], dy_send.at[j - 1], dy_recv.at[j - 1], (me, to)
-            ))
-    for c in copies:
-        c.wait()
-
-    def finish(i, carry):
-        r = pl.ds(pl.multiple_of(i * 64, 64), 64)
-        s = pd[tp, r, :].astype(F32)
-        for j in range(ny - 1):
-            s = s + part[r, (ny + j) * span:(ny + j + 1) * span].astype(F32)
-        out_ref[r, :] = (mixed[r, pl.ds(pl.multiple_of(tp * span, span), span)].astype(F32) + s).astype(BF16)
-        return carry
-
-    lax.fori_loop(0, rows // 64, finish, 0)
+        lax.fori_loop(0, half // tile, merge, 0, unroll=2)
+        to, local, slot = target(owner)
+
+        @pl.when(to != tp)
+        def _():
+            remote(pd.at[owner, mine_rows], inbox.at[local, slot], out_send.at[d], out_recv.at[local, slot], (me, to))
+
+    waiting = None
+    for d in order:
+        serve(need[d] - done[0])
+        c = lower(d)
+        if waiting is not None:
+            reduce(*waiting)
+        waiting = (d, c)
+    reduce(*waiting)
+    serve(len(queue))
+
+    span = per_tp * block
+    for local in range(per_tp):
+        owner = tp * per_tp + local
+        for slot in range(ntp - 1):
+            ref = inbox.at[local, slot]
+            pltpu.make_async_remote_copy(
+                src_ref=ref, dst_ref=ref, send_sem=out_send.at[0], recv_sem=out_recv.at[local, slot],
+                device_id=(me, partner), device_id_type=MESH,
+            ).wait_recv()
+        for same in range(2):
+            base = (core if same else 1 - core) * half
+            slots = range(1, ntp - 1, 2) if same else range(0, ntp - 1, 2)
+
+            def finish(i, carry):
+                r = pl.ds(pl.multiple_of(i * tile, tile), tile)
+                o = pl.ds(pl.multiple_of(base + i * tile, tile), tile)
+                s = sum(inbox[local, slot, r, :].astype(F32) for slot in slots)
+                if same:
+                    s = s + pd[owner, o, :].astype(F32)
+                kept = mixed[o, pl.ds(pl.multiple_of(tp * span, span), span)]
+                kept = kept[:, local * block:(local + 1) * block].astype(F32)
+                out_ref[o, local * block:(local + 1) * block] = (kept + s).astype(BF16)
+                return carry
+
+            lax.fori_loop(0, half // tile, finish, 0)
+    for d in range(n):
+        owner = place(lax.rem(pos + d, n))
+        to, local, slot = target(owner)
+
+        @pl.when(to != tp)
+        def _():
+            ref = pd.at[owner, mine_rows]
+            pltpu.make_async_remote_copy(
+                src_ref=ref, dst_ref=ref, send_sem=out_send.at[d], recv_sem=out_recv.at[0, 0],
+                device_id=(me, to), device_id_type=MESH,
+            ).wait_send()
     for stream in range(4):
         for way in range(2):
             for s in range(n - 1):
                 ring(stream, way, s, False).wait_send()
-
-
-def second_in(ref, slot, span):
-    return ref.at[:, pl.ds(pl.multiple_of(slot * span, span), span)]
 
 
 def solution(mesh):
@@ -357,15 +400,8 @@
         hidden = wv.shape[1]
         block = wv.shape[0]
         ny = ntp // 2
-        edge_fwd = [(i, i + 1) for i in range(n - 1)]
-        edge_bwd = [(b, a) for a, b in edge_fwd]
         labels = doc + 1
-        before = lax.ppermute(labels[-1:], "sp", edge_fwd)
-        after = lax.ppermute(labels[:1], "sp", edge_bwd)
-        padded = jnp.concatenate([before, labels, after])
-        prev_ok = (padded[:-2] == labels).astype(F32)[:, None]
-        next_ok = (padded[2:] == labels).astype(F32)[:, None]
-        lab_row = jnp.broadcast_to(labels[None, :], (8, rows))
+        lab_row = labels[None, :]
         vm = pl.BlockSpec(memory_space=pltpu.VMEM)
         hbm = pl.BlockSpec(memory_space=pl.ANY)
         smem = pl.BlockSpec(memory_space=pltpu.SMEM)
@@ -377,7 +413,8 @@
             pltpu.VMEM((n * block, hidden), BF16),
             pltpu.VMEM((rows + 2 * WINDOW, kvc), BF16),
             pltpu.VMEM((rows + 2 * WINDOW, kvc), BF16),
-            pltpu.VMEM((8, rows + 2 * WINDOW), jnp.int32),
+            pltpu.VMEM((1, rows + 2 * WINDOW), jnp.int32),
+            pltpu.VMEM((rows + 2 * WINDOW, WINDOW), F32),
             pltpu.VMEM((rows, model), BF16),
             pltpu.VMEM((rows // 2, model), BF16),
             pltpu.VMEM((max(ny - 1, 1), rows // 2 // ny, model), BF16),
@@ -386,7 +423,9 @@
             pltpu.VMEM((rows, hidden), BF16),
             pltpu.VMEM((rows, hidden), BF16),
             pltpu.VMEM((2, RIM, hidden), BF16),
-            pltpu.VMEM((ntp, rows, span), BF16),
+            pltpu.VMEM((n, rows, block), BF16),
+            pltpu.VMEM((n, rows // 2, block), BF16),
+            pltpu.VMEM((n // ntp, ntp - 1, rows // 2, block), BF16),
             pltpu.VMEM((rows // 2 // ny, model), BF16),
             dma((4,)),
             dma((4, 2, n - 1)), dma((4, 2, n - 1)),
@@ -396,20 +435,20 @@
             dma((ny,)), dma((ny,)),
             dma((ny,)), dma((ny,)),
             dma, dma,
-            dma((ny,)), dma((ny,)),
-            dma((ny,)), dma((ny,)),
+            dma((n,)), dma((n,)),
+            dma((n,)), dma((n // ntp, ntp - 1)),
         ]
         return pl.pallas_call(
             functools.partial(kernel, n, ntp),
             out_shape=jax.ShapeDtypeStruct((rows, span), BF16),
-            in_specs=[vm, vm, vm, smem, vm, vm, vm, vm, hbm, vm, vm, hbm, hbm, vm, hbm],
+            in_specs=[vm, vm, vm, smem, vm, hbm, vm, vm, hbm, hbm, vm, hbm],
             out_specs=vm,
             scratch_shapes=scratch,
             compiler_params=pltpu.CompilerParams(
                 collective_id=0, has_side_effects=True, vmem_limit_bytes=67043328
             ),
             name="layer",
-        )(q, k, v, sink, lab_row, labels[:, None], prev_ok, next_ok, res, wout, gain[None, :], wv, wg, taps, wd)
+        )(q, k, v, sink, lab_row, res, wout, gain[None, :], wv, wg, taps, wd)
 
     placed = (
         P("sp", "tp"), P("sp", "tp"), P("sp", "tp"), P("tp"), P("sp"), P("sp", None),

time: 226 us -> 202 us (0.89)
  Pallas kernels: 209 us -> 199 us
  starting transfers between devices: 7.28 us -> 0 us
  local copies, waits for them, and re-layouts: 6.02 us -> 2.65 us
    pallas_call x1, Pallas kernels: 209 us -> 199 us  [per_device(): pl.pallas_call(functools.partial(kernel, n, ntp), out_shape=jax.ShapeDtyp...]
    ppermute x2 -> x0, starting transfers between devices: 7.28 us -> none  [the longest x1 6 us: per_device(): before = lax.ppermute(labels[-1:], 'sp', edge_fwd)]
    broadcast_in_dim x4 -> x1, local copies, waits for them, and re-layouts: 3.38 us -> 0.58 us  [per_device(): lab_row = labels[None, :]]
  transfers between devices with their start and end apart: 2 -> 0, of which waited for: 1 -> 0; matrix products, arithmetic and copies ran while one was open for 0% -> 0% of each run, Pallas kernels for 0% -> 0%
where the time goes in v2:
time: 202 us
  Pallas kernels  199 us (99%)
  local copies, waits for them, and re-layouts  2.65 us (1%)
    pallas_call x1, Pallas kernels, per_device(): pl.pallas_call(functools.partial(kernel, n, ntp), out_shape=jax.ShapeDtyp...  199 us

profile of v2, /device:TPU:0, one launch (start us, length us, event | category | flops | bytes accessed | tf_op | source)
XLA Modules:
  0.0 202.2 jit_solution(15982230473250026476)
XLA Ops:
  0.0 0.7 broadcast_add_fusion
  0.7 0.6 broadcast_in_dim.6.lab_row_ref
  1.3 198.9 %layer.1 = bf16[768,512]{1,0:T(8,128)(2,1)} custom-call(bf16[768,512]{1,0:T(8,128)(2,1)} %q_ref.1, bf16[768,128]{1,0:T(8,128)(2,1)} %k_ref.1, bf16[768,128]{1,0:T(8,128)(2,1)} %v_ref.1, f32[8]{0:T(128)} %sink_ref.1, s32[1,768]{1,0:T(1,128)} %broadcast_in_dim.6.lab_row_ref, bf16[768,2048]{1,0:T(8,128)(2,1)} %res_hbm.1, bf16[512,2048]{1,0:T(8,128)(2,1)} %wout_ref.1, ...), custom_call_target="tpu_custom_call" | custom-call | tf_op jit(solution)/shard_map/layer/pallas_call | solution.py:441
  200.2 2.1 %copy.14 = bf16[768,512]{1,0:T(8,128)(2,1)} copy(bf16[768,512]{1,0:T(8,128)(2,1)} %layer.1) | data formatting | bytes 1572864

commit v3 on v2

--- a/solution.py
+++ b/solution.py
@@ -188,7 +188,7 @@
     split = blocks // 3
     for t in range(3):
         lax.fori_loop(t * split, (t + 1) * split if t < 2 else blocks, attend, 0)
-        serve(1)
+        serve(2 if t == 1 else 1)
 
     tile = 32
     other_half = pl.ds((1 - core) * half, half)
@@ -292,14 +292,20 @@
         )
         gate[r, :] = (conv * jax.nn.sigmoid(conv) * gate[r, :].astype(F32)).astype(BF16)
         before = x[step - 1:step]
-        if i % 4 == 3:
+        if i % 3 == 2:
             serve(1)
 
     per_tp = n // ntp
     mine_rows = pl.ds(core * half, half)
     partner_rows = pl.ds((1 - core) * half, half)
-    need = {d: 2 * (n - 1) + (2 * max(d, n - d) if d else 0) for d in range(n)}
-    order = sorted(range(n), key=lambda d: need[d])
+    units = []
+    for d in range(n):
+        if d in (1, n - 1) and n > 2:
+            units.append((2 * (n - 1) + 2 * (n - d), d, 0, 1))
+            units.append((2 * (n - 1) + 2 * d, d, 1, 1))
+        else:
+            units.append((2 * (n - 1) + (2 * max(d, n - d) if d else 0), d, 0, 2))
+    units.sort()
 
     def target(owner):
         to = owner // per_tp
@@ -307,30 +313,36 @@
         slot = lax.rem(tp - to + ntp, ntp) - 1
         return to, local, slot
 
-    def lower(d):
+    def lower(u):
+        _, d, way, count = units[u]
         owner = place(lax.rem(pos + d, n))
-        w = down[pl.ds(pl.multiple_of(owner * block, block), block), :]
+        w = down[pl.ds(pl.multiple_of(owner * block + way * depth, depth), count * depth), :]
 
         def body(i, carry):
             r = pl.ds(pl.multiple_of(i * big, big), big)
-            pd[owner, r, :] = lax.dot_general(
+            product = lax.dot_general(
                 gate[r, :], w, (((1,), (1,)), ((), ())), preferred_element_type=F32
             ).astype(BF16)
+            for j in range(count):
+                pd[owner, way + j, r, :] = product[:, j * depth:(j + 1) * depth]
             return carry
 
         lax.fori_loop(0, 3, body, 0)
         return remote(
-            pd.at[owner, partner_rows], box.at[owner], down_send.at[d], down_recv.at[d], (me, partner)
+            pd.at[owner, pl.ds(way, count), partner_rows], box.at[owner, pl.ds(way, count)],
+            down_send.at[u], down_recv.at[u], (me, partner),
         )
 
-    def reduce(d, c):
+    def reduce(u, c):
+        _, d, way, count = units[u]
         owner = place(lax.rem(pos + d, n))
         c.wait()
 
         def merge(i, carry):
             r = pl.ds(pl.multiple_of(i * tile, tile), tile)
             o = pl.ds(pl.multiple_of(core * half + i * tile, tile), tile)
-            pd[owner, o, :] = (pd[owner, o, :].astype(F32) + box[owner, r, :].astype(F32)).astype(BF16)
+            for j in range(way, way + count):
+                pd[owner, j, o, :] = (pd[owner, j, o, :].astype(F32) + box[owner, j, r, :].astype(F32)).astype(BF16)
             return carry
 
         lax.fori_loop(0, half // tile, merge, 0, unroll=2)
@@ -338,15 +350,18 @@
 
         @pl.when(to != tp)
         def _():
-            remote(pd.at[owner, mine_rows], inbox.at[local, slot], out_send.at[d], out_recv.at[local, slot], (me, to))
+            remote(
+                pd.at[owner, pl.ds(way, count), mine_rows], inbox.at[local, slot, pl.ds(way, count)],
+                out_send.at[u], out_recv.at[local, slot], (me, to),
+            )
 
     waiting = None
-    for d in order:
-        serve(need[d] - done[0])
-        c = lower(d)
+    for u in range(len(units)):
+        serve(units[u][0] - done[0])
+        c = lower(u)
         if waiting is not None:
             reduce(*waiting)
-        waiting = (d, c)
+        waiting = (u, c)
     reduce(*waiting)
     serve(len(queue))
 
@@ -366,24 +381,25 @@
             def finish(i, carry):
                 r = pl.ds(pl.multiple_of(i * tile, tile), tile)
                 o = pl.ds(pl.multiple_of(base + i * tile, tile), tile)
-                s = sum(inbox[local, slot, r, :].astype(F32) for slot in slots)
-                if same:
-                    s = s + pd[owner, o, :].astype(F32)
                 kept = mixed[o, pl.ds(pl.multiple_of(tp * span, span), span)]
-                kept = kept[:, local * block:(local + 1) * block].astype(F32)
-                out_ref[o, local * block:(local + 1) * block] = (kept + s).astype(BF16)
+                for j in range(2):
+                    s = sum(inbox[local, slot, j, r, :].astype(F32) for slot in slots)
+                    if same:
+                        s = s + pd[owner, j, o, :].astype(F32)
+                    cols = slice(local * block + j * depth, local * block + (j + 1) * depth)
+                    out_ref[o, cols] = (kept[:, cols].astype(F32) + s).astype(BF16)
                 return carry
 
             lax.fori_loop(0, half // tile, finish, 0)
-    for d in range(n):
+    for u, (_, d, way, count) in enumerate(units):
         owner = place(lax.rem(pos + d, n))
         to, local, slot = target(owner)
 
         @pl.when(to != tp)
         def _():
-            ref = pd.at[owner, mine_rows]
+            ref = pd.at[owner, pl.ds(way, count), mine_rows]
             pltpu.make_async_remote_copy(
-                src_ref=ref, dst_ref=ref, send_sem=out_send.at[d], recv_sem=out_recv.at[0, 0],
+                src_ref=ref, dst_ref=ref, send_sem=out_send.at[u], recv_sem=out_recv.at[0, 0],
                 device_id=(me, to), device_id_type=MESH,
             ).wait_send()
     for stream in range(4):
@@ -423,9 +439,9 @@
             pltpu.VMEM((rows, hidden), BF16),
             pltpu.VMEM((rows, hidden), BF16),
             pltpu.VMEM((2, RIM, hidden), BF16),
-            pltpu.VMEM((n, rows, block), BF16),
-            pltpu.VMEM((n, rows // 2, block), BF16),
-            pltpu.VMEM((n // ntp, ntp - 1, rows // 2, block), BF16),
+            pltpu.VMEM((n, 2, rows, block // 2), BF16),
+            pltpu.VMEM((n, 2, rows // 2, block // 2), BF16),
+            pltpu.VMEM((n // ntp, ntp - 1, 2, rows // 2, block // 2), BF16),
             pltpu.VMEM((rows // 2 // ny, model), BF16),
             dma((4,)),
             dma((4, 2, n - 1)), dma((4, 2, n - 1)),
@@ -435,8 +451,8 @@
             dma((ny,)), dma((ny,)),
             dma((ny,)), dma((ny,)),
             dma, dma,
-            dma((n,)), dma((n,)),
-            dma((n,)), dma((n // ntp, ntp - 1)),
+            dma((n + 2,)), dma((n + 2,)),
+            dma((n + 2,)), dma((n // ntp, ntp - 1)),
         ]
         return pl.pallas_call(
             functools.partial(kernel, n, ntp),

time: 202 us -> 200 us (0.990)
  Pallas kernels: 199 us -> 196 us
    pallas_call x1, Pallas kernels: 199 us -> 196 us  [per_device(): pl.pallas_call(functools.partial(kernel, n, ntp), out_shape=jax.ShapeDtyp...]
where the time goes in v3:
time: 200 us
  Pallas kernels  196 us (98%)
  local copies, waits for them, and re-layouts  2.65 us (1%)
    pallas_call x1, Pallas kernels, per_device(): pl.pallas_call(functools.partial(kernel, n, ntp), out_shape=jax.ShapeDtyp...  196 us

profile of v3, /device:TPU:0, one launch (start us, length us, event | category | flops | bytes accessed | tf_op | source)
XLA Modules:
  0.0 199.8 jit_solution(15652527315017378975)
XLA Ops:
  0.0 0.7 broadcast_add_fusion
  0.7 0.6 broadcast_in_dim.6.lab_row_ref
  1.3 196.4 %layer.1 = bf16[768,512]{1,0:T(8,128)(2,1)} custom-call(bf16[768,512]{1,0:T(8,128)(2,1)} %q_ref.1, bf16[768,128]{1,0:T(8,128)(2,1)} %k_ref.1, bf16[768,128]{1,0:T(8,128)(2,1)} %v_ref.1, f32[8]{0:T(128)} %sink_ref.1, s32[1,768]{1,0:T(1,128)} %broadcast_in_dim.6.lab_row_ref, bf16[768,2048]{1,0:T(8,128)(2,1)} %res_hbm.1, bf16[512,2048]{1,0:T(8,128)(2,1)} %wout_ref.1, ...), custom_call_target="tpu_custom_call" | custom-call | tf_op jit(solution)/shard_map/layer/pallas_call | solution.py:457
  197.7 2.1 %copy.14 = bf16[768,512]{1,0:T(8,128)(2,1)} copy(bf16[768,512]{1,0:T(8,128)(2,1)} %layer.1) | data formatting | bytes 1572864
